TPU v7x, 32 devices: a whole 2x2x4 slice. The times are simulated.
32 devices in a mesh: sp: 16 (over z, y, x), tp: 2 (over core).
Axes of the slice: x: 2, y: 2, z: 4, core: 2. Of those that a mesh axis runs over, the one named last changes fastest.
Arguments:
- queries: bfloat16 [4096, 512], P('sp', 'tp'), may hold values from -6 to 6
- keys: bfloat16 [4096, 512], P('sp', 'tp'), may hold values from -6 to 6
- values: bfloat16 [4096, 512], P('sp', 'tp'), may hold values from -6 to 6
- gains: float32 [2, 128], replicated, may hold values from 0.1 to 1.9
- bias_table: float32 [192, 4], P(None, 'tp'), may hold values from -6 to 270
- d_out: bfloat16 [4096, 512], P('sp', 'tp'), may hold values from -32 to 32
Outputs:
- d_queries: bfloat16 [4096, 512], P('sp', 'tp')
- d_keys: bfloat16 [4096, 512], P('sp', 'tp')
- d_values: bfloat16 [4096, 512], P('sp', 'tp')
- d_table: float32 [192, 4], P(None, 'tp')
- d_gains: float32 [2, 128], replicated
All inputs are finite; a program needn't handle non-finite values.
Results may differ from a plain program's by a relative error of at most 0.008.
Values may be sent and summed in bfloat16 or wider, within the bound.
No kernel may reach another device: no remote copies, remote signals or barrier semaphores. Data moves between devices by JAX's collectives and lax.ppermute only.
A program may use at most 64 MiB of HBM per device.

v0:
```python
import jax
import jax.numpy as jnp
from jax import lax
from jax.experimental import pallas as pl
from jax.experimental.pallas import tpu as pltpu
from jax.sharding import PartitionSpec as P


HEAD_DIM = 128
SEG = 64
LEFT = 4
MAX_REL = 128
ENTRIES = MAX_REL + SEG
EPSILON = 1e-06
FACTOR = HEAD_DIM ** (-0.5)
TAIL = LEFT * SEG

BLOCK = 2 * SEG
WINDOW = LEFT // 2 + 1
PREV = WINDOW - 1
MASKED = -1e30

F32 = jnp.float32
BF16 = jnp.bfloat16


def dot(a, b, contract):
    return lax.dot_general(a, b, ((contract[:1], contract[1:]), ((), ())), preferred_element_type=F32)


def shifted(block, distance):
    size = lax.axis_size("sp")
    return lax.ppermute(block, "sp", [(i, (i + distance) % size) for i in range(size)])


def unit_rows(rows):
    rows = rows.astype(F32)
    inv_rms = lax.rsqrt(jnp.mean(rows * rows, axis=-1, keepdims=True) + EPSILON)
    return rows * inv_rms, inv_rms


def rows_back(d_normed, unit, inv_rms, gain):
    g = d_normed * gain
    return inv_rms * (g - unit * jnp.mean(g * unit, axis=-1, keepdims=True))


def lanes(shape):
    return lax.broadcasted_iota(jnp.int32, shape, len(shape) - 1)


def toeplitz(row):
    base = pltpu.roll(jnp.broadcast_to(row, (8, 2 * BLOCK)), 0, 1, stride=1, stride_axis=0)
    tiles = [base[:, :BLOCK]]
    for a in range(8, BLOCK, 8):
        tiles.append(pltpu.roll(base, a, 1)[:, :BLOCK])
    return jnp.concatenate(tiles, axis=0)


def diagonals(tile):
    width = 2 * BLOCK
    total = jnp.zeros((8, width), F32)
    empty = jnp.zeros((8, BLOCK), F32)
    for a in range(0, BLOCK, 8):
        part = jnp.concatenate([tile[a : a + 8], empty], axis=1)
        total = total + (pltpu.roll(part, width - a, 1) if a else part)
    out = total[:1]
    for s in range(1, 8):
        out = out + pltpu.roll(total, width - s, 1)[s : s + 1]
    return out


def bias_blocks(table):
    width = 2 * BLOCK
    last = table[:, ENTRIES - 1 :]
    lane = lanes((1, width))
    wide = jnp.concatenate([table, jnp.zeros((1, width - ENTRIES), F32)], axis=1)
    far = jnp.broadcast_to(last, (BLOCK, BLOCK))
    middle = toeplitz(jnp.where(lane < BLOCK, last, pltpu.roll(wide, width - (ENTRIES - 1), 1)))
    near = toeplitz(pltpu.roll(wide, width - (SEG - 1), 1))
    key = lax.broadcasted_iota(jnp.int32, (BLOCK, BLOCK), 0)
    query = lax.broadcasted_iota(jnp.int32, (BLOCK, BLOCK), 1)
    far = jnp.where((key < SEG) & (query >= SEG), MASKED, far)
    near = jnp.where((key >= SEG) & (query < SEG), MASKED, near)
    return [far, middle, near]


def table_row(far, middle, near):
    width = 2 * BLOCK
    lane = lanes((1, width))
    mid = diagonals(middle)
    last = jnp.sum(far) + jnp.sum(jnp.where(lane < BLOCK, mid, 0.0))
    mid = jnp.where(lane < BLOCK, 0.0, mid)
    row = pltpu.roll(diagonals(near), SEG - 1, 1) + pltpu.roll(mid, ENTRIES - 1, 1)
    return row + jnp.where(lane == ENTRIES - 1, last, 0.0)


def add(total, value):
    return value if total is None else total + value


def columns(h):
    return slice(h * HEAD_DIM, (h + 1) * HEAD_DIM)


def block_rows(b):
    return slice(b * BLOCK, (b + 1) * BLOCK)


def pair_lists(blocks):
    pairs = [(p, w) for p in range(blocks) for w in range(WINDOW)]
    return [x for x in pairs if sum(x) < PREV], [x for x in pairs if sum(x) >= PREV]


def own_kernel(
    q_hbm, k_hbm, v_hbm, do_hbm, gains_hbm, table_hbm,
    do_ref, gains_ref, qn_ref, qu_ref, qr_ref, kn_ref, ku_ref, kr_ref, bias_ref, e_ref, dp_ref, stat_ref,
    q_ref, k_ref, v_ref, table_ref, sems,
):
    moves = [(table_hbm, table_ref), (gains_hbm, gains_ref), (q_hbm, q_ref), (k_hbm, k_ref), (v_hbm, v_ref), (do_hbm, do_ref)]
    copies = [pltpu.make_async_copy(a, b, sems.at[i]) for i, (a, b) in enumerate(moves)]
    for copy in copies:
        copy.start()
    for copy in copies:
        copy.wait()
    rows, features = q_ref.shape
    blocks = rows // BLOCK
    _, own = pair_lists(blocks)
    first = lax.axis_index("sp") == 0
    for h in range(features // HEAD_DIM):
        cols = columns(h)
        q_unit, q_rms = unit_rows(q_ref[:, cols])
        k_unit, k_rms = unit_rows(k_ref[:, cols])
        q_norm = (q_unit * gains_ref[0:1]).astype(BF16)
        k_norm = (k_unit * gains_ref[1:2]).astype(BF16)
        qn_ref[:, cols], kn_ref[:, cols] = q_norm, k_norm
        qu_ref[:, cols], ku_ref[:, cols] = q_unit, k_unit
        qr_ref[:, cols] = jnp.broadcast_to(q_rms, q_unit.shape)
        kr_ref[:, cols] = jnp.broadcast_to(k_rms, k_unit.shape)
        bias = bias_blocks(table_ref[h : h + 1])
        for w in range(PREV):
            bias_ref[h, w] = jnp.where(first, MASKED, bias[w])
        for p in range(blocks):
            mine = [(i, w) for i, (pp, w) in enumerate(own) if pp == p]
            keys = slice((p + mine[0][1] - PREV) * BLOCK, (p + 1) * BLOCK)
            at = block_rows(p)
            s = dot(k_norm[keys], q_norm[at], (1, 1)) * FACTOR
            s = s + jnp.concatenate([bias[w] for _, w in mine], axis=0)
            top = jnp.max(s, axis=0, keepdims=True)
            e = jnp.exp(s - top)
            d_prob = dot(v_ref[keys, cols], do_ref[at, cols], (1, 1))
            for n, (i, _) in enumerate(mine):
                e_ref[h, i] = e[block_rows(n)]
                dp_ref[h, i] = d_prob[block_rows(n)]
            stat_ref[h, 2 * p : 2 * p + 1] = top
            stat_ref[h, 2 * p + 1 : 2 * p + 2] = jnp.sum(e, axis=0, keepdims=True)


def keys_kernel(
    pk_ref, qn_ref, do_ref, gains_ref, bias_ref, e_ref, stat_ref,
    pkn_ref, pku_ref, pp_ref, po_ref, back_ref, dv_ref,
):
    rows, features = qn_ref.shape
    blocks = rows // BLOCK
    prev, own = pair_lists(blocks)
    for h in range(features // HEAD_DIM):
        cols = columns(h)
        k_unit, _ = unit_rows(pk_ref[:, cols])
        k_norm = (k_unit * gains_ref[1:2]).astype(BF16)
        pkn_ref[:, cols], pku_ref[:, cols] = k_norm, k_unit
        dv = [None] * (blocks + PREV)
        for p in range(blocks):
            at = block_rows(p)
            top_own, sum_own = stat_ref[h, 2 * p : 2 * p + 1], stat_ref[h, 2 * p + 1 : 2 * p + 2]
            before = [(i, w) for i, (pp, w) in enumerate(prev) if pp == p]
            mine = [(i, w) for i, (pp, w) in enumerate(own) if pp == p]
            probs = {}
            if before:
                s = dot(k_norm[p * BLOCK :], qn_ref[at, cols], (1, 1)) * FACTOR
                s = s + jnp.concatenate([bias_ref[h, w] for _, w in before], axis=0)
                top = jnp.maximum(top_own, jnp.max(s, axis=0, keepdims=True))
                e = jnp.exp(s - top)
                scale = jnp.exp(top_own - top)
                inverse = 1.0 / (sum_own * scale + jnp.sum(e, axis=0, keepdims=True))
                for n, (i, w) in enumerate(before):
                    probs[w] = e[block_rows(n)] * inverse
                    pp_ref[h, i] = probs[w]
                scale = scale * inverse
            else:
                scale = 1.0 / sum_own
            for i, w in mine:
                probs[w] = e_ref[h, i] * scale
                po_ref[h, i] = probs[w]
            prob_low = jnp.concatenate([probs[w].astype(BF16) for w in range(WINDOW)], axis=0)
            dv_w = dot(prob_low, do_ref[at, cols], (1, 0))
            for w in range(WINDOW):
                dv[p + w] = add(dv[p + w], dv_w[block_rows(w)])
        for b in range(PREV):
            back_ref[block_rows(b), cols] = dv[b].astype(BF16)
        for b in range(blocks):
            dv_ref[block_rows(b), cols] = dv[PREV + b]


def values_kernel(
    pv_ref, pp_ref, po_ref, dpo_ref, do_ref, qn_ref, kn_ref, pkn_ref, qu_ref, ku_ref, pku_ref, dvb_ref,
    dq_ref, back_ref, dk_ref, parts_ref,
):
    rows, features = qn_ref.shape
    heads = features // HEAD_DIM
    blocks = rows // BLOCK
    prev, own = pair_lists(blocks)
    cells = [(h, p) for h in range(heads) for p in range(blocks)]
    d_score, d_low, pieces = {}, {}, []
    new = {}
    for h, p in cells:
        if any(pp == p for pp, _ in prev):
            new[h, p] = dot(pv_ref[p * BLOCK :, columns(h)], do_ref[block_rows(p), columns(h)], (1, 1))
    for h, p in cells:
        probs, d_probs, n = [], [], 0
        for w in range(WINDOW):
            if p + w < PREV:
                i = prev.index((p, w))
                probs.append(pp_ref[h, i])
                d_probs.append(new[h, p][block_rows(n)])
                n += 1
            else:
                i = own.index((p, w))
                probs.append(po_ref[h, i])
                d_probs.append(dpo_ref[h, i])
        delta = sum(jnp.sum(a * b, axis=0, keepdims=True) for a, b in zip(probs, d_probs))
        d_score[h, p] = [a * (b - delta) for a, b in zip(probs, d_probs)]
        d_low[h, p] = jnp.concatenate([d.astype(BF16) for d in d_score[h, p]], axis=0)
    dk = [[None] * (blocks + PREV) for _ in range(heads)]
    for h, p in cells:
        dk_w = dot(d_low[h, p], qn_ref[block_rows(p), columns(h)], (1, 0))
        for w in range(WINDOW):
            dk[h][p + w] = add(dk[h][p + w], dk_w[block_rows(w)])
    d_gain_q = jnp.zeros((1, HEAD_DIM), F32)
    d_gain_k = jnp.zeros((1, HEAD_DIM), F32)
    for h, p in cells:
        at, cols = block_rows(p), columns(h)
        k_w = [pkn_ref[block_rows(e), cols] if e < PREV else kn_ref[block_rows(e - PREV), cols] for e in range(p, p + WINDOW)]
        dq = dot(d_low[h, p], jnp.concatenate(k_w, axis=0), (0, 0)) * FACTOR
        d_gain_q = d_gain_q + jnp.sum(dq * qu_ref[at, cols], axis=0, keepdims=True)
        dq_ref[at, cols] = dq
    for h in range(heads):
        band = [sum(d_score[h, p][w] for p in range(blocks)) for w in range(WINDOW)]
        row = table_row(*band)
        pieces += [row[:, :HEAD_DIM], row[:, HEAD_DIM:]]
    for h in range(heads):
        cols = columns(h)
        for b in range(blocks + PREV):
            d_here = dk[h][b] * FACTOR
            if b < PREV:
                unit = pku_ref[block_rows(b), cols]
                back_ref[block_rows(b), cols] = d_here.astype(BF16)
                back_ref[block_rows(PREV + b), cols] = dvb_ref[block_rows(b), cols]
            else:
                unit = ku_ref[block_rows(b - PREV), cols]
                dk_ref[block_rows(b - PREV), cols] = d_here
            d_gain_k = d_gain_k + jnp.sum(d_here * unit, axis=0, keepdims=True)
    pieces += [d_gain_q, d_gain_k]
    count = parts_ref.shape[1]
    pieces += [jnp.zeros((count - len(pieces), HEAD_DIM), F32)]
    parts_ref[...] = jnp.broadcast_to(jnp.concatenate(pieces, axis=0)[None], parts_ref.shape)


def final_kernel(
    dq_ref, dk_ref, dv_ref, back_ref, qu_ref, qr_ref, ku_ref, kr_ref, gains_ref, parts_ref,
    dq_out, dk_out, dv_out, dt_ref, dg_ref,
):
    rows, features = dk_ref.shape
    heads = features // HEAD_DIM
    sp, tp = lax.axis_size("sp"), lax.axis_size("tp")
    for h in range(heads):
        cols = columns(h)
        for b in range(rows // BLOCK):
            at = block_rows(b)
            dq_out[at, cols] = rows_back(
                dq_ref[at, cols], qu_ref[at, cols], qr_ref[at, cols], gains_ref[0:1]
            ).astype(BF16)
            dk, dv = dk_ref[at, cols], dv_ref[at, cols]
            from_end = b - (rows - TAIL) // BLOCK
            if from_end >= 0:
                dk = dk + back_ref[block_rows(from_end), cols].astype(F32)
                dv = dv + back_ref[block_rows(PREV + from_end), cols].astype(F32)
            dk_out[at, cols] = rows_back(dk, ku_ref[at, cols], kr_ref[at, cols], gains_ref[1:2]).astype(BF16)
            dv_out[at, cols] = dv.astype(BF16)
    parts = parts_ref[...]
    parts = jnp.sum(parts.reshape(sp, tp, *parts.shape[1:]), axis=0)
    mine = parts[0]
    for i in range(1, tp):
        mine = jnp.where(lax.axis_index("tp") == i, parts[i], mine)
    for h in range(heads):
        row = jnp.concatenate([mine[2 * h : 2 * h + 1], mine[2 * h + 1 : 2 * h + 2]], axis=1)
        dt_ref[h : h + 1, :] = row[:, :ENTRIES]
    dg_ref[...] = jnp.sum(parts, axis=0)[2 * heads : 2 * heads + 2]


def call(kernel, name, outs, *operands, **options):
    place = jax.ShapeDtypeStruct if name == "final" else pltpu.VMEM
    return pl.pallas_call(
        kernel,
        out_shape=tuple(place(*o) for o in outs),
        **options,
        compiler_params=pltpu.CompilerParams(vmem_limit_bytes=12 << 20),
    )(*operands)


def local(queries, keys, values, gains, bias_table, d_out):
    rows, features = queries.shape
    heads = features // HEAD_DIM
    blocks = rows // BLOCK
    prev, own = (len(x) for x in pair_lists(blocks))
    members = lax.axis_size("sp") * lax.axis_size("tp")
    count = -(-(2 * heads + 2) // 8) * 8
    wide, low = ((rows, features), F32), ((rows, features), BF16)
    tail, tail_low = ((TAIL, features), F32), ((TAIL, features), BF16)
    tiles = lambda n: ((heads, n, BLOCK, BLOCK), F32)

    prev_k = shifted(keys[rows - TAIL :], 1)
    prev_v = shifted(values[rows - TAIL :], 1)
    do, g, qn, qu, qr, kn, ku, kr, bias, e_own, dp_own, stats = call(
        own_kernel, "own",
        (low, ((2, HEAD_DIM), F32), low, wide, wide, low, wide, wide, tiles(PREV), tiles(own), tiles(own),
         ((heads, 2 * blocks, BLOCK), F32)),
        *(pltpu.with_memory_space_constraint(x, pltpu.HBM) for x in (queries, keys, values, d_out, gains, bias_table.T)),
        in_specs=[pl.BlockSpec(memory_space=pltpu.HBM)] * 6,
        scratch_shapes=[pltpu.VMEM(*low)] * 3
        + [pltpu.VMEM((heads, ENTRIES), F32), pltpu.SemaphoreType.DMA((6,))],
    )
    pkn, pku, p_prev, p_own, back_v, dv_own = call(
        keys_kernel, "keys", (tail_low, tail, tiles(prev), tiles(own), tail_low, wide),
        prev_k, qn, do, g, bias, e_own, stats,
    )
    dq, back, dk_own, parts = call(
        values_kernel, "values", (wide, ((2 * TAIL, features), BF16), wide, ((members, count, HEAD_DIM), F32)),
        prev_v, p_prev, p_own, dp_own, do, qn, kn, pkn, qu, ku, pku, back_v,
    )
    back = shifted(back, -1)
    parts = lax.all_to_all(parts, ("sp", "tp"), 0, 0)
    d_queries, d_keys, d_values, d_table, d_gains = call(
        final_kernel, "final", (low, low, low, ((heads, ENTRIES), F32), ((2, HEAD_DIM), F32)),
        dq, dk_own, dv_own, back, qu, qr, ku, kr, g, parts,
    )
    return d_queries, d_keys, d_values, d_table.T, d_gains


def solution(mesh):
    in_specs = (P("sp", "tp"), P("sp", "tp"), P("sp", "tp"), P(), P(None, "tp"), P("sp", "tp"))
    out_specs = (P("sp", "tp"), P("sp", "tp"), P("sp", "tp"), P(None, "tp"), P())
    return jax.shard_map(local, mesh=mesh, in_specs=in_specs, out_specs=out_specs, check_vma=False)
```

profile of v0, /device:TPU:0, one launch (start us, length us, event | category | flops | bytes accessed | tf_op | source)
XLA Modules:
  0.0 27.6 jit_solution(1505942792899974628)
XLA Ops:
  0.6 3.0 %collective-permute-start.1 = (bf16[256,256]{1,0:T(8,128)(2,1)}, bf16[256,256]{1,0:T(8,128)(2,1)S(1)}, u32[]{:S(2)}, u32[]{:S(2)}) collective-permute-start(bf16[256,256]{1,0:T(8,128)(2,1)} %k_hbm.1), channel_id=1, source_target_pairs={{0,2},{2,4},{4,6},{6,8},{8,10},{10,12},{12,14},{14,16},{16,18},{18... | collective-permute-start | bytes 393224 | tf_op jit(solution)/shard_map/ppermute | solution.py:33
  3.7 1.5 %collective-permute-start = (bf16[256,256]{1,0:T(8,128)(2,1)}, bf16[256,256]{1,0:T(8,128)(2,1)S(1)}, u32[]{:S(2)}, u32[]{:S(2)}) collective-permute-start(bf16[256,256]{1,0:T(8,128)(2,1)} %v_hbm.1), channel_id=1, source_target_pairs={{0,2},{2,4},{4,6},{6,8},{8,10},{10,12},{12,14},{14,16},{16,18},{18... | collective-permute-start | bytes 393224 | tf_op jit(solution)/shard_map/ppermute | solution.py:33
  5.1 1.8 %shard_map.101 = (bf16[256,256]{1,0:T(8,128)(2,1)S(1)}, f32[2,128]{1,0:T(2,128)S(1)}, bf16[256,256]{1,0:T(8,128)(2,1)S(1)}, f32[256,256]{1,0:T(8,128)S(1)}, f32[...) custom-call(bf16[256,256]{1,0:T(8,128)(2,1)} %q_hbm.1, ...), custom_call_target="tpu_custom_call" | custom-call | tf_op jit(solution)/shard_map/pallas_call | solution.py:301
  7.0 5.2 %collective-permute-done.1.pk_ref = bf16[256,256]{1,0:T(8,128)(2,1)S(1)} collective-permute-done((bf16[256,256]{1,0:T(8,128)(2,1)}, bf16[256,256]{1,0:T(8,128)(2,1)S(1)}, u32[]{:S(2)}, u32[]{:S(2)}) %collective-permute-start.1) | collective-permute-done | bytes 131104 | tf_op jit(solution)/shard_map/ppermute | solution.py:33
  12.2 0.8 %shard_map.102 = (bf16[256,256]{1,0:T(8,128)(2,1)S(1)}, f32[256,256]{1,0:T(8,128)S(1)}, f32[2,3,128,128]{3,2,1,0:T(8,128)S(1)}, f32[2,3,128,128]{3,2,1,0:T(8,128...) custom-call(bf16[256,256]{1,0:T(8,128)(2,1)S(1)} %collective-permute-done.1.pk_ref, ...), custom_call_target="tpu_custom_call" | custom-call | tf_op jit(solution)/shard_map/pallas_call | solution.py:301
  13.0 1.1 %collective-permute-done.pv_ref = bf16[256,256]{1,0:T(8,128)(2,1)S(1)} collective-permute-done((bf16[256,256]{1,0:T(8,128)(2,1)}, bf16[256,256]{1,0:T(8,128)(2,1)S(1)}, u32[]{:S(2)}, u32[]{:S(2)}) %collective-permute-start) | collective-permute-done | bytes 131104 | tf_op jit(solution)/shard_map/ppermute | solution.py:33
  14.2 0.8 %shard_map.103 = (f32[256,256]{1,0:T(8,128)S(1)}, bf16[512,256]{1,0:T(8,128)(2,1)S(1)}, f32[256,256]{1,0:T(8,128)S(1)}, f32[32,8,128]{2,1,0:T(8,128)S(1)}) custom-call(bf16[256,256]{1,0:T(8,128)(2,1)S(1)} %collective-permute-done.pv_ref, f32[2,3,128,128]{3,2,1,0:T(8,128)S(1)} %get-tuple-element.38.pp_ref, f32[2,3,128,128]{3,2,1,0:T(8,128)S(1)} %get-tuple-element.39.po_ref, ...), custom_call_target="tpu_custom_call" | custom-call | tf_op jit(solution)/shard_map/pallas_call | solution.py:301
  15.0 1.8 %collective-permute-start.2 = (bf16[512,256]{1,0:T(8,128)(2,1)S(1)}, bf16[512,256]{1,0:T(8,128)(2,1)S(1)}, u32[]{:S(2)}, u32[]{:S(2)}) collective-permute-start(bf16[512,256]{1,0:T(8,128)(2,1)S(1)} %get-tuple-element.50), channel_id=1, source_target_pairs={{0,30},{2,0},{4,2},{6,4},{8,6},{10,8},{12,10},{14,12},{16,14},{18,... | collective-permute-start | bytes 786440 | tf_op jit(solution)/shard_map/ppermute | solution.py:33
  16.8 9.9 %all_to_all.5.parts_ref = f32[32,8,128]{2,1,0:T(8,128)S(1)} all-to-all(f32[32,8,128]{2,1,0:T(8,128)S(1)} %get-tuple-element.53), channel_id=1, replica_groups=mesh['sp'=16,'tp'=2] {'sp','tp'}, dimensions={0} | all-to-all | bytes 262144 | tf_op jit(solution)/shard_map/all_to_all | solution.py:340
  26.7 0.0 collective-permute-done.2.back_ref
  26.7 1.0 %shard_map.104 = (bf16[256,256]{1,0:T(8,128)(2,1)}, bf16[256,256]{1,0:T(8,128)(2,1)}, bf16[256,256]{1,0:T(8,128)(2,1)}, f32[2,192]{1,0:T(2,128)}, f32[2,128]{1,0:T(2,128)}) custom-call(f32[256,256]{1,0:T(8,128)S(1)} %get-tuple-element.47.dq_ref, f32[256,256]{1,0:T(8,128)S(1)} %get-tuple-element.48.dk_ref, f32[256,256]{1,0:T(8,128)S(1)} %get-tuple-element.49.dv_ref, ...), custom_call_target="tpu_custom_call" | custom-call | tf_op jit(solution)/shard_map/pallas_call | solution.py:301
Async XLA Ops:
  0.6 11.6 %collective-permute-start.1 = (bf16[256,256]{1,0:T(8,128)(2,1)}, bf16[256,256]{1,0:T(8,128)(2,1)S(1)}, u32[]{:S(2)}, u32[]{:S(2)}) collective-permute-start(bf16[256,256]{1,0:T(8,128)(2,1)} %k_hbm.1), channel_id=1, source_target_pairs={{0,2},{2,4},{4,6},{6,8},{8,10},{10,12},{12,14},{14,16},{16,18},{18... | collective-permute-start | bytes 393224 | tf_op jit(solution)/shard_map/ppermute | solution.py:33
  3.7 10.5 %collective-permute-start = (bf16[256,256]{1,0:T(8,128)(2,1)}, bf16[256,256]{1,0:T(8,128)(2,1)S(1)}, u32[]{:S(2)}, u32[]{:S(2)}) collective-permute-start(bf16[256,256]{1,0:T(8,128)(2,1)} %v_hbm.1), channel_id=1, source_target_pairs={{0,2},{2,4},{4,6},{6,8},{8,10},{10,12},{12,14},{14,16},{16,18},{18... | collective-permute-start | bytes 393224 | tf_op jit(solution)/shard_map/ppermute | solution.py:33
  15.0 11.7 %collective-permute-start.2 = (bf16[512,256]{1,0:T(8,128)(2,1)S(1)}, bf16[512,256]{1,0:T(8,128)(2,1)S(1)}, u32[]{:S(2)}, u32[]{:S(2)}) collective-permute-start(bf16[512,256]{1,0:T(8,128)(2,1)S(1)} %get-tuple-element.50), channel_id=1, source_target_pairs={{0,30},{2,0},{4,2},{6,4},{8,6},{10,8},{12,10},{14,12},{16,14},{18,... | collective-permute-start | bytes 786440 | tf_op jit(solution)/shard_map/ppermute | solution.py:33
where the time goes:
time: 27.8 us; the launch traced here: 27.6 us
  blocking collectives  9.89 us (36%)
  waiting for transfers between devices  6.33 us (23%)
  starting transfers between devices  6.3 us (23%)
  Pallas kernels  4.45 us (16%)
  between operations  0.65 us (2%)
    all_to_all x1, blocking collectives, local(): parts = lax.all_to_all(parts, ('sp', 'tp'), 0, 0)  9.89 us
    ppermute x3, waiting for transfers between devices, shifted(): lax.ppermute(block, 'sp', [(i, (i + distance) % size) for i in range(size)])  6.33 us
    ppermute x3, starting transfers between devices, shifted(): lax.ppermute(block, 'sp', [(i, (i + distance) % size) for i in range(size)])  6.3 us
    pallas_call x4, Pallas kernels, call(): pl.pallas_call(kernel, out_shape=tuple((place(*o) for o in outs)), **opti...  4.45 us
  transfers between devices with their start and end apart: 3, of which 2 were waited for; matrix products, arithmetic and copies ran while one was open for 0% of the time, Pallas kernels for 10%

commit v1 on v0

--- a/solution.py
+++ b/solution.py
@@ -162,42 +162,51 @@
     rows, features = qn_ref.shape
     blocks = rows // BLOCK
     prev, own = pair_lists(blocks)
-    for h in range(features // HEAD_DIM):
-        cols = columns(h)
-        k_unit, _ = unit_rows(pk_ref[:, cols])
-        k_norm = (k_unit * gains_ref[1:2]).astype(BF16)
-        pkn_ref[:, cols], pku_ref[:, cols] = k_norm, k_unit
-        dv = [None] * (blocks + PREV)
-        for p in range(blocks):
-            at = block_rows(p)
-            top_own, sum_own = stat_ref[h, 2 * p : 2 * p + 1], stat_ref[h, 2 * p + 1 : 2 * p + 2]
-            before = [(i, w) for i, (pp, w) in enumerate(prev) if pp == p]
-            mine = [(i, w) for i, (pp, w) in enumerate(own) if pp == p]
-            probs = {}
-            if before:
-                s = dot(k_norm[p * BLOCK :], qn_ref[at, cols], (1, 1)) * FACTOR
-                s = s + jnp.concatenate([bias_ref[h, w] for _, w in before], axis=0)
-                top = jnp.maximum(top_own, jnp.max(s, axis=0, keepdims=True))
-                e = jnp.exp(s - top)
-                scale = jnp.exp(top_own - top)
-                inverse = 1.0 / (sum_own * scale + jnp.sum(e, axis=0, keepdims=True))
-                for n, (i, w) in enumerate(before):
-                    probs[w] = e[block_rows(n)] * inverse
-                    pp_ref[h, i] = probs[w]
-                scale = scale * inverse
+    heads = features // HEAD_DIM
+    cells = [(h, p) for h in range(heads) for p in range(blocks)]
+    joined = [(h, p) for h, p in cells if p < PREV]
+    k_norm, s, scale = {}, {}, {}
+    for h in range(heads):
+        k_unit, _ = unit_rows(pk_ref[:, columns(h)])
+        k_norm[h] = (k_unit * gains_ref[1:2]).astype(BF16)
+        pkn_ref[:, columns(h)], pku_ref[:, columns(h)] = k_norm[h], k_unit
+    for h, p in joined:
+        s[h, p] = dot(k_norm[h][p * BLOCK :], qn_ref[block_rows(p), columns(h)], (1, 1))
+    prob = {}
+    for h, p in cells:
+        top_own, sum_own = stat_ref[h, 2 * p : 2 * p + 1], stat_ref[h, 2 * p + 1 : 2 * p + 2]
+        scale = 1.0
+        total = sum_own
+        if (h, p) in joined:
+            bias = jnp.concatenate([bias_ref[h, w] for w in range(PREV - p)], axis=0)
+            scores = s[h, p] * FACTOR + bias
+            top = jnp.maximum(top_own, jnp.max(scores, axis=0, keepdims=True))
+            e = jnp.exp(scores - top)
+            scale = jnp.exp(top_own - top)
+            total = sum_own * scale + jnp.sum(e, axis=0, keepdims=True)
+        inverse = 1.0 / total
+        scale = scale * inverse
+        parts = []
+        for w in range(WINDOW):
+            if p + w < PREV:
+                i = prev.index((p, w))
+                parts.append(e[block_rows(w)] * inverse)
+                pp_ref[h, i] = parts[w]
             else:
-                scale = 1.0 / sum_own
-            for i, w in mine:
-                probs[w] = e_ref[h, i] * scale
-                po_ref[h, i] = probs[w]
-            prob_low = jnp.concatenate([probs[w].astype(BF16) for w in range(WINDOW)], axis=0)
-            dv_w = dot(prob_low, do_ref[at, cols], (1, 0))
-            for w in range(WINDOW):
-                dv[p + w] = add(dv[p + w], dv_w[block_rows(w)])
+                i = own.index((p, w))
+                parts.append(e_ref[h, i] * scale)
+                po_ref[h, i] = parts[w]
+        prob[h, p] = jnp.concatenate([x.astype(BF16) for x in parts], axis=0)
+    dv = [[None] * (blocks + PREV) for _ in range(heads)]
+    for h, p in cells:
+        dv_w = dot(prob[h, p], do_ref[block_rows(p), columns(h)], (1, 0))
+        for w in range(WINDOW):
+            dv[h][p + w] = add(dv[h][p + w], dv_w[block_rows(w)])
+    for h in range(heads):
         for b in range(PREV):
-            back_ref[block_rows(b), cols] = dv[b].astype(BF16)
+            back_ref[block_rows(b), columns(h)] = dv[h][b].astype(BF16)
         for b in range(blocks):
-            dv_ref[block_rows(b), cols] = dv[PREV + b]
+            dv_ref[block_rows(b), columns(h)] = dv[h][PREV + b]
 
 
 def values_kernel(
@@ -245,7 +254,7 @@
     for h in range(heads):
         band = [sum(d_score[h, p][w] for p in range(blocks)) for w in range(WINDOW)]
         row = table_row(*band)
-        pieces += [row[:, :HEAD_DIM], row[:, HEAD_DIM:]]
+        pieces.append(row[:, :ENTRIES])
     for h in range(heads):
         cols = columns(h)
         for b in range(blocks + PREV):
@@ -258,10 +267,13 @@
                 unit = ku_ref[block_rows(b - PREV), cols]
                 dk_ref[block_rows(b - PREV), cols] = d_here
             d_gain_k = d_gain_k + jnp.sum(d_here * unit, axis=0, keepdims=True)
-    pieces += [d_gain_q, d_gain_k]
-    count = parts_ref.shape[1]
-    pieces += [jnp.zeros((count - len(pieces), HEAD_DIM), F32)]
-    parts_ref[...] = jnp.broadcast_to(jnp.concatenate(pieces, axis=0)[None], parts_ref.shape)
+    width = parts_ref.shape[2]
+    gap = width - heads * ENTRIES - 2 * HEAD_DIM
+    pieces += ([jnp.zeros((1, gap), F32)] if gap else []) + [d_gain_q, d_gain_k]
+    flat = jnp.concatenate(pieces, axis=1)
+    for c in range(0, width, HEAD_DIM):
+        at = slice(c, c + HEAD_DIM)
+        parts_ref[:, :, at] = jnp.broadcast_to(flat[None, :, at], (parts_ref.shape[0], 1, HEAD_DIM))
 
 
 def final_kernel(
@@ -270,7 +282,7 @@
 ):
     rows, features = dk_ref.shape
     heads = features // HEAD_DIM
-    sp, tp = lax.axis_size("sp"), lax.axis_size("tp")
+    tp = lax.axis_size("tp")
     for h in range(heads):
         cols = columns(h)
         for b in range(rows // BLOCK):
@@ -285,15 +297,19 @@
                 dv = dv + back_ref[block_rows(PREV + from_end), cols].astype(F32)
             dk_out[at, cols] = rows_back(dk, ku_ref[at, cols], kr_ref[at, cols], gains_ref[1:2]).astype(BF16)
             dv_out[at, cols] = dv.astype(BF16)
-    parts = parts_ref[...]
-    parts = jnp.sum(parts.reshape(sp, tp, *parts.shape[1:]), axis=0)
-    mine = parts[0]
+    members = parts_ref.shape[0]
+    width = parts_ref.shape[2]
+    sums = [parts_ref[i] for i in range(tp)]
+    for n in range(tp, members):
+        sums[n % tp] = sums[n % tp] + parts_ref[n]
+    mine, total = sums[0], sums[0]
     for i in range(1, tp):
-        mine = jnp.where(lax.axis_index("tp") == i, parts[i], mine)
-    for h in range(heads):
-        row = jnp.concatenate([mine[2 * h : 2 * h + 1], mine[2 * h + 1 : 2 * h + 2]], axis=1)
-        dt_ref[h : h + 1, :] = row[:, :ENTRIES]
-    dg_ref[...] = jnp.sum(parts, axis=0)[2 * heads : 2 * heads + 2]
+        mine = jnp.where(lax.axis_index("tp") == i, sums[i], mine)
+        total = total + sums[i]
+    for h in range(heads):
+        dt_ref[h : h + 1, :] = mine[:, h * ENTRIES : (h + 1) * ENTRIES]
+    dg_ref[0:1] = total[:, width - 2 * HEAD_DIM : width - HEAD_DIM]
+    dg_ref[1:2] = total[:, width - HEAD_DIM :]
 
 
 def call(kernel, name, outs, *operands, **options):
@@ -312,7 +328,7 @@
     blocks = rows // BLOCK
     prev, own = (len(x) for x in pair_lists(blocks))
     members = lax.axis_size("sp") * lax.axis_size("tp")
-    count = -(-(2 * heads + 2) // 8) * 8
+    width = (-(-heads * ENTRIES // HEAD_DIM) + 2) * HEAD_DIM
     wide, low = ((rows, features), F32), ((rows, features), BF16)
     tail, tail_low = ((TAIL, features), F32), ((TAIL, features), BF16)
     tiles = lambda n: ((heads, n, BLOCK, BLOCK), F32)
@@ -333,7 +349,7 @@
         prev_k, qn, do, g, bias, e_own, stats,
     )
     dq, back, dk_own, parts = call(
-        values_kernel, "values", (wide, ((2 * TAIL, features), BF16), wide, ((members, count, HEAD_DIM), F32)),
+        values_kernel, "values", (wide, ((2 * TAIL, features), BF16), wide, ((members, 1, width), F32)),
         prev_v, p_prev, p_own, dp_own, do, qn, kn, pkn, qu, ku, pku, back_v,
     )
     back = shifted(back, -1)

time: 27.8 us -> 27.2 us (0.978)
  blocking collectives: 9.89 us -> 9.26 us
    all_to_all x1, blocking collectives: 9.89 us -> 9.26 us  [local(): parts = lax.all_to_all(parts, ('sp', 'tp'), 0, 0)]
  transfers between devices with their start and end apart: 3 -> 3, of which waited for: 2 -> 2; matrix products, arithmetic and copies ran while one was open for 0% -> 0% of each run, Pallas kernels for 10% -> 9%
where the time goes in v1:
time: 27.2 us; the launch traced here: 27 us
  blocking collectives  9.26 us (34%)
  waiting for transfers between devices  6.55 us (24%)
  starting transfers between devices  6.3 us (23%)
  Pallas kernels  4.25 us (16%)
  between operations  0.65 us (2%)
    all_to_all x1, blocking collectives, local(): parts = lax.all_to_all(parts, ('sp', 'tp'), 0, 0)  9.26 us
    ppermute x3, waiting for transfers between devices, shifted(): lax.ppermute(block, 'sp', [(i, (i + distance) % size) for i in range(size)])  6.55 us
    ppermute x3, starting transfers between devices, shifted(): lax.ppermute(block, 'sp', [(i, (i + distance) % size) for i in range(size)])  6.3 us
    pallas_call x4, Pallas kernels, call(): pl.pallas_call(kernel, out_shape=tuple((place(*o) for o in outs)), **opti...  4.25 us
  transfers between devices with their start and end apart: 3, of which 2 were waited for; matrix products, arithmetic and copies ran while one was open for 0% of the time, Pallas kernels for 9%

profile of v1, /device:TPU:0, one launch (start us, length us, event | category | flops | bytes accessed | tf_op | source)
XLA Modules:
  0.0 27.0 jit_solution(542060858616031669)
XLA Ops:
  0.6 3.0 %collective-permute-start.1 = (bf16[256,256]{1,0:T(8,128)(2,1)}, bf16[256,256]{1,0:T(8,128)(2,1)S(1)}, u32[]{:S(2)}, u32[]{:S(2)}) collective-permute-start(bf16[256,256]{1,0:T(8,128)(2,1)} %k_hbm.1), channel_id=1, source_target_pairs={{0,2},{2,4},{4,6},{6,8},{8,10},{10,12},{12,14},{14,16},{16,18},{18... | collective-permute-start | bytes 393224 | tf_op jit(solution)/shard_map/ppermute | solution.py:33
  3.7 1.5 %collective-permute-start = (bf16[256,256]{1,0:T(8,128)(2,1)}, bf16[256,256]{1,0:T(8,128)(2,1)S(1)}, u32[]{:S(2)}, u32[]{:S(2)}) collective-permute-start(bf16[256,256]{1,0:T(8,128)(2,1)} %v_hbm.1), channel_id=1, source_target_pairs={{0,2},{2,4},{4,6},{6,8},{8,10},{10,12},{12,14},{14,16},{16,18},{18... | collective-permute-start | bytes 393224 | tf_op jit(solution)/shard_map/ppermute | solution.py:33
  5.1 1.8 %shard_map.101 = (bf16[256,256]{1,0:T(8,128)(2,1)S(1)}, f32[2,128]{1,0:T(2,128)S(1)}, bf16[256,256]{1,0:T(8,128)(2,1)S(1)}, f32[256,256]{1,0:T(8,128)S(1)}, f32[...) custom-call(bf16[256,256]{1,0:T(8,128)(2,1)} %q_hbm.1, ...), custom_call_target="tpu_custom_call" | custom-call | tf_op jit(solution)/shard_map/pallas_call | solution.py:317
  7.0 5.2 %collective-permute-done.1.pk_ref = bf16[256,256]{1,0:T(8,128)(2,1)S(1)} collective-permute-done((bf16[256,256]{1,0:T(8,128)(2,1)}, bf16[256,256]{1,0:T(8,128)(2,1)S(1)}, u32[]{:S(2)}, u32[]{:S(2)}) %collective-permute-start.1) | collective-permute-done | bytes 131104 | tf_op jit(solution)/shard_map/ppermute | solution.py:33
  12.2 0.6 %shard_map.102 = (bf16[256,256]{1,0:T(8,128)(2,1)S(1)}, f32[256,256]{1,0:T(8,128)S(1)}, f32[2,3,128,128]{3,2,1,0:T(8,128)S(1)}, f32[2,3,128,128]{3,2,1,0:T(8,128...) custom-call(bf16[256,256]{1,0:T(8,128)(2,1)S(1)} %collective-permute-done.1.pk_ref, ...), custom_call_target="tpu_custom_call" | custom-call | tf_op jit(solution)/shard_map/pallas_call | solution.py:317
  12.8 1.3 %collective-permute-done.pv_ref = bf16[256,256]{1,0:T(8,128)(2,1)S(1)} collective-permute-done((bf16[256,256]{1,0:T(8,128)(2,1)}, bf16[256,256]{1,0:T(8,128)(2,1)S(1)}, u32[]{:S(2)}, u32[]{:S(2)}) %collective-permute-start) | collective-permute-done | bytes 131104 | tf_op jit(solution)/shard_map/ppermute | solution.py:33
  14.2 0.8 %shard_map.103 = (f32[256,256]{1,0:T(8,128)S(1)}, bf16[512,256]{1,0:T(8,128)(2,1)S(1)}, f32[256,256]{1,0:T(8,128)S(1)}, f32[32,1,640]{2,1,0:T(1,128)S(1)}) custom-call(bf16[256,256]{1,0:T(8,128)(2,1)S(1)} %collective-permute-done.pv_ref, f32[2,3,128,128]{3,2,1,0:T(8,128)S(1)} %get-tuple-element.38.pp_ref, f32[2,3,128,128]{3,2,1,0:T(8,128)S(1)} %get-tuple-element.39.po_ref, ...), custom_call_target="tpu_custom_call" | custom-call | tf_op jit(solution)/shard_map/pallas_call | solution.py:317
  15.0 1.8 %collective-permute-start.2 = (bf16[512,256]{1,0:T(8,128)(2,1)S(1)}, bf16[512,256]{1,0:T(8,128)(2,1)S(1)}, u32[]{:S(2)}, u32[]{:S(2)}) collective-permute-start(bf16[512,256]{1,0:T(8,128)(2,1)S(1)} %get-tuple-element.50), channel_id=1, source_target_pairs={{0,30},{2,0},{4,2},{6,4},{8,6},{10,8},{12,10},{14,12},{16,14},{18,... | collective-permute-start | bytes 786440 | tf_op jit(solution)/shard_map/ppermute | solution.py:33
  16.8 9.3 %all_to_all.5.parts_ref = f32[32,1,640]{2,1,0:T(1,128)S(1)} all-to-all(f32[32,1,640]{2,1,0:T(1,128)S(1)} %get-tuple-element.53), channel_id=1, replica_groups=mesh['sp'=16,'tp'=2] {'sp','tp'}, dimensions={0} | all-to-all | bytes 163840 | tf_op jit(solution)/shard_map/all_to_all | solution.py:356
  26.0 0.0 collective-permute-done.2.back_ref
  26.0 1.0 %shard_map.104 = (bf16[256,256]{1,0:T(8,128)(2,1)}, bf16[256,256]{1,0:T(8,128)(2,1)}, bf16[256,256]{1,0:T(8,128)(2,1)}, f32[2,192]{1,0:T(2,128)}, f32[2,128]{1,0:T(2,128)}) custom-call(f32[256,256]{1,0:T(8,128)S(1)} %get-tuple-element.47.dq_ref, f32[256,256]{1,0:T(8,128)S(1)} %get-tuple-element.48.dk_ref, f32[256,256]{1,0:T(8,128)S(1)} %get-tuple-element.49.dv_ref, ...), custom_call_target="tpu_custom_call" | custom-call | tf_op jit(solution)/shard_map/pallas_call | solution.py:317
Async XLA Ops:
  0.6 11.6 %collective-permute-start.1 = (bf16[256,256]{1,0:T(8,128)(2,1)}, bf16[256,256]{1,0:T(8,128)(2,1)S(1)}, u32[]{:S(2)}, u32[]{:S(2)}) collective-permute-start(bf16[256,256]{1,0:T(8,128)(2,1)} %k_hbm.1), channel_id=1, source_target_pairs={{0,2},{2,4},{4,6},{6,8},{8,10},{10,12},{12,14},{14,16},{16,18},{18... | collective-permute-start | bytes 393224 | tf_op jit(solution)/shard_map/ppermute | solution.py:33
  3.7 10.5 %collective-permute-start = (bf16[256,256]{1,0:T(8,128)(2,1)}, bf16[256,256]{1,0:T(8,128)(2,1)S(1)}, u32[]{:S(2)}, u32[]{:S(2)}) collective-permute-start(bf16[256,256]{1,0:T(8,128)(2,1)} %v_hbm.1), channel_id=1, source_target_pairs={{0,2},{2,4},{4,6},{6,8},{8,10},{10,12},{12,14},{14,16},{16,18},{18... | collective-permute-start | bytes 393224 | tf_op jit(solution)/shard_map/ppermute | solution.py:33
  15.0 11.1 %collective-permute-start.2 = (bf16[512,256]{1,0:T(8,128)(2,1)S(1)}, bf16[512,256]{1,0:T(8,128)(2,1)S(1)}, u32[]{:S(2)}, u32[]{:S(2)}) collective-permute-start(bf16[512,256]{1,0:T(8,128)(2,1)S(1)} %get-tuple-element.50), channel_id=1, source_target_pairs={{0,30},{2,0},{4,2},{6,4},{8,6},{10,8},{12,10},{14,12},{16,14},{18,... | collective-permute-start | bytes 786440 | tf_op jit(solution)/shard_map/ppermute | solution.py:33

commit v2 on v1

--- a/solution.py
+++ b/solution.py
@@ -204,13 +204,13 @@
             dv[h][p + w] = add(dv[h][p + w], dv_w[block_rows(w)])
     for h in range(heads):
         for b in range(PREV):
-            back_ref[block_rows(b), columns(h)] = dv[h][b].astype(BF16)
+            back_ref[block_rows(PREV + b), columns(h)] = dv[h][b].astype(BF16)
         for b in range(blocks):
             dv_ref[block_rows(b), columns(h)] = dv[h][PREV + b]
 
 
 def values_kernel(
-    pv_ref, pp_ref, po_ref, dpo_ref, do_ref, qn_ref, kn_ref, pkn_ref, qu_ref, ku_ref, pku_ref, dvb_ref,
+    pv_ref, pp_ref, po_ref, dpo_ref, do_ref, qn_ref, kn_ref, pkn_ref, qu_ref, ku_ref, pku_ref, _,
     dq_ref, back_ref, dk_ref, parts_ref,
 ):
     rows, features = qn_ref.shape
@@ -262,18 +262,17 @@
             if b < PREV:
                 unit = pku_ref[block_rows(b), cols]
                 back_ref[block_rows(b), cols] = d_here.astype(BF16)
-                back_ref[block_rows(PREV + b), cols] = dvb_ref[block_rows(b), cols]
             else:
                 unit = ku_ref[block_rows(b - PREV), cols]
                 dk_ref[block_rows(b - PREV), cols] = d_here
             d_gain_k = d_gain_k + jnp.sum(d_here * unit, axis=0, keepdims=True)
-    width = parts_ref.shape[2]
-    gap = width - heads * ENTRIES - 2 * HEAD_DIM
+    gap = -heads * ENTRIES % HEAD_DIM
     pieces += ([jnp.zeros((1, gap), F32)] if gap else []) + [d_gain_q, d_gain_k]
     flat = jnp.concatenate(pieces, axis=1)
-    for c in range(0, width, HEAD_DIM):
-        at = slice(c, c + HEAD_DIM)
-        parts_ref[:, :, at] = jnp.broadcast_to(flat[None, :, at], (parts_ref.shape[0], 1, HEAD_DIM))
+    lines = [flat[:, c : c + HEAD_DIM] for c in range(0, flat.shape[1], HEAD_DIM)]
+    once = jnp.concatenate(lines * 8, axis=0)
+    for r in range(0, parts_ref.shape[0], once.shape[0]):
+        parts_ref[r : r + once.shape[0]] = once
 
 
 def final_kernel(
@@ -345,15 +344,15 @@
         + [pltpu.VMEM((heads, ENTRIES), F32), pltpu.SemaphoreType.DMA((6,))],
     )
     pkn, pku, p_prev, p_own, back_v, dv_own = call(
-        keys_kernel, "keys", (tail_low, tail, tiles(prev), tiles(own), tail_low, wide),
+        keys_kernel, "keys", (tail_low, tail, tiles(prev), tiles(own), ((2 * TAIL, features), BF16), wide),
         prev_k, qn, do, g, bias, e_own, stats,
     )
     dq, back, dk_own, parts = call(
-        values_kernel, "values", (wide, ((2 * TAIL, features), BF16), wide, ((members, 1, width), F32)),
-        prev_v, p_prev, p_own, dp_own, do, qn, kn, pkn, qu, ku, pku, back_v,
+        values_kernel, "values", (wide, ((2 * TAIL, features), BF16), wide, ((members * width // HEAD_DIM, HEAD_DIM), F32)),
+        prev_v, p_prev, p_own, dp_own, do, qn, kn, pkn, qu, ku, pku, back_v, input_output_aliases={11: 1},
     )
     back = shifted(back, -1)
-    parts = lax.all_to_all(parts, ("sp", "tp"), 0, 0)
+    parts = lax.all_to_all(parts.reshape(members, 1, width), ("sp", "tp"), 0, 0)
     d_queries, d_keys, d_values, d_table, d_gains = call(
         final_kernel, "final", (low, low, low, ((heads, ENTRIES), F32), ((2, HEAD_DIM), F32)),
         dq, dk_own, dv_own, back, qu, qr, ku, kr, g, parts,

time: 27.2 us -> 27.2 us (level)
  no operation moved by 1% of the time
where the time goes in v2:
time: 27.2 us; the launch traced here: 27 us
  blocking collectives  9.26 us (34%)
  waiting for transfers between devices  6.55 us (24%)
  starting transfers between devices  6.3 us (23%)
  Pallas kernels  4.22 us (16%)
  between operations  0.65 us (2%)
    all_to_all x1, blocking collectives, local(): parts = lax.all_to_all(parts.reshape(members, 1, width), ('sp', 'tp'), 0, 0)  9.26 us
    ppermute x3, waiting for transfers between devices, shifted(): lax.ppermute(block, 'sp', [(i, (i + distance) % size) for i in range(size)])  6.55 us
    ppermute x3, starting transfers between devices, shifted(): lax.ppermute(block, 'sp', [(i, (i + distance) % size) for i in range(size)])  6.3 us
    pallas_call x4, Pallas kernels, call(): pl.pallas_call(kernel, out_shape=tuple((place(*o) for o in outs)), **opti...  4.22 us
  transfers between devices with their start and end apart: 3, of which 2 were waited for; matrix products, arithmetic and copies ran while one was open for 0% of the time, Pallas kernels for 9%

profile of v2, /device:TPU:0, one launch (start us, length us, event | category | flops | bytes accessed | tf_op | source)
XLA Modules:
  0.0 27.0 jit_solution(12010072469992395916)
XLA Ops:
  0.6 3.0 %collective-permute-start.1 = (bf16[256,256]{1,0:T(8,128)(2,1)}, bf16[256,256]{1,0:T(8,128)(2,1)S(1)}, u32[]{:S(2)}, u32[]{:S(2)}) collective-permute-start(bf16[256,256]{1,0:T(8,128)(2,1)} %k_hbm.1), channel_id=1, source_target_pairs={{0,2},{2,4},{4,6},{6,8},{8,10},{10,12},{12,14},{14,16},{16,18},{18... | collective-permute-start | bytes 393224 | tf_op jit(solution)/shard_map/ppermute | solution.py:33
  3.7 1.5 %collective-permute-start = (bf16[256,256]{1,0:T(8,128)(2,1)}, bf16[256,256]{1,0:T(8,128)(2,1)S(1)}, u32[]{:S(2)}, u32[]{:S(2)}) collective-permute-start(bf16[256,256]{1,0:T(8,128)(2,1)} %v_hbm.1), channel_id=1, source_target_pairs={{0,2},{2,4},{4,6},{6,8},{8,10},{10,12},{12,14},{14,16},{16,18},{18... | collective-permute-start | bytes 393224 | tf_op jit(solution)/shard_map/ppermute | solution.py:33
  5.1 1.8 %shard_map.101 = (bf16[256,256]{1,0:T(8,128)(2,1)S(1)}, f32[2,128]{1,0:T(2,128)S(1)}, bf16[256,256]{1,0:T(8,128)(2,1)S(1)}, f32[256,256]{1,0:T(8,128)S(1)}, f32[...) custom-call(bf16[256,256]{1,0:T(8,128)(2,1)} %q_hbm.1, ...), custom_call_target="tpu_custom_call" | custom-call | tf_op jit(solution)/shard_map/pallas_call | solution.py:316
  7.0 5.2 %collective-permute-done.1.pk_ref = bf16[256,256]{1,0:T(8,128)(2,1)S(1)} collective-permute-done((bf16[256,256]{1,0:T(8,128)(2,1)}, bf16[256,256]{1,0:T(8,128)(2,1)S(1)}, u32[]{:S(2)}, u32[]{:S(2)}) %collective-permute-start.1) | collective-permute-done | bytes 131104 | tf_op jit(solution)/shard_map/ppermute | solution.py:33
  12.2 0.6 %shard_map.102 = (bf16[256,256]{1,0:T(8,128)(2,1)S(1)}, f32[256,256]{1,0:T(8,128)S(1)}, f32[2,3,128,128]{3,2,1,0:T(8,128)S(1)}, f32[2,3,128,128]{3,2,1,0:T(8,128...) custom-call(bf16[256,256]{1,0:T(8,128)(2,1)S(1)} %collective-permute-done.1.pk_ref, ...), custom_call_target="tpu_custom_call" | custom-call | tf_op jit(solution)/shard_map/pallas_call | solution.py:316
  12.8 1.3 %collective-permute-done.pv_ref = bf16[256,256]{1,0:T(8,128)(2,1)S(1)} collective-permute-done((bf16[256,256]{1,0:T(8,128)(2,1)}, bf16[256,256]{1,0:T(8,128)(2,1)S(1)}, u32[]{:S(2)}, u32[]{:S(2)}) %collective-permute-start) | collective-permute-done | bytes 131104 | tf_op jit(solution)/shard_map/ppermute | solution.py:33
  14.2 0.8 %shard_map.103 = (f32[256,256]{1,0:T(8,128)S(1)}, bf16[512,256]{1,0:T(8,128)(2,1)S(1)}, f32[256,256]{1,0:T(8,128)S(1)}, f32[160,128]{1,0:T(8,128)S(1)}) custom-call(bf16[256,256]{1,0:T(8,128)(2,1)S(1)} %collective-permute-done.pv_ref, f32[2,3,128,128]{3,2,1,0:T(8,128)S(1)} %get-tuple-element.38.pp_ref, ...), custom_call_target="tpu_custom_call", output_to_operand_aliasing={{1}: (11, {})} | custom-call | tf_op jit(solution)/shard_map/pallas_call | solution.py:316
  15.0 1.8 %collective-permute-start.2 = (bf16[512,256]{1,0:T(8,128)(2,1)S(1)}, bf16[512,256]{1,0:T(8,128)(2,1)S(1)}, u32[]{:S(2)}, u32[]{:S(2)}) collective-permute-start(bf16[512,256]{1,0:T(8,128)(2,1)S(1)} %get-tuple-element.50), channel_id=1, source_target_pairs={{0,30},{2,0},{4,2},{6,4},{8,6},{10,8},{12,10},{14,12},{16,14},{18,... | collective-permute-start | bytes 786440 | tf_op jit(solution)/shard_map/ppermute | solution.py:33
  16.7 9.3 %all_to_all.5.parts_ref = f32[32,1,640]{2,1,0:T(1,128)S(1)} all-to-all(f32[32,1,640]{2,1,0:T(1,128)S(1)} %bitcast.3), channel_id=1, replica_groups=mesh['sp'=16,'tp'=2] {'sp','tp'}, dimensions={0} | all-to-all | bytes 163840 | tf_op jit(solution)/shard_map/all_to_all | solution.py:355
  26.0 0.0 collective-permute-done.2.back_ref
  26.0 1.0 %shard_map.104 = (bf16[256,256]{1,0:T(8,128)(2,1)}, bf16[256,256]{1,0:T(8,128)(2,1)}, bf16[256,256]{1,0:T(8,128)(2,1)}, f32[2,192]{1,0:T(2,128)}, f32[2,128]{1,0:T(2,128)}) custom-call(f32[256,256]{1,0:T(8,128)S(1)} %get-tuple-element.47.dq_ref, f32[256,256]{1,0:T(8,128)S(1)} %get-tuple-element.48.dk_ref, f32[256,256]{1,0:T(8,128)S(1)} %get-tuple-element.49.dv_ref, ...), custom_call_target="tpu_custom_call" | custom-call | tf_op jit(solution)/shard_map/pallas_call | solution.py:316
Async XLA Ops:
  0.6 11.6 %collective-permute-start.1 = (bf16[256,256]{1,0:T(8,128)(2,1)}, bf16[256,256]{1,0:T(8,128)(2,1)S(1)}, u32[]{:S(2)}, u32[]{:S(2)}) collective-permute-start(bf16[256,256]{1,0:T(8,128)(2,1)} %k_hbm.1), channel_id=1, source_target_pairs={{0,2},{2,4},{4,6},{6,8},{8,10},{10,12},{12,14},{14,16},{16,18},{18... | collective-permute-start | bytes 393224 | tf_op jit(solution)/shard_map/ppermute | solution.py:33
  3.7 10.5 %collective-permute-start = (bf16[256,256]{1,0:T(8,128)(2,1)}, bf16[256,256]{1,0:T(8,128)(2,1)S(1)}, u32[]{:S(2)}, u32[]{:S(2)}) collective-permute-start(bf16[256,256]{1,0:T(8,128)(2,1)} %v_hbm.1), channel_id=1, source_target_pairs={{0,2},{2,4},{4,6},{6,8},{8,10},{10,12},{12,14},{14,16},{16,18},{18... | collective-permute-start | bytes 393224 | tf_op jit(solution)/shard_map/ppermute | solution.py:33
  15.0 11.1 %collective-permute-start.2 = (bf16[512,256]{1,0:T(8,128)(2,1)S(1)}, bf16[512,256]{1,0:T(8,128)(2,1)S(1)}, u32[]{:S(2)}, u32[]{:S(2)}) collective-permute-start(bf16[512,256]{1,0:T(8,128)(2,1)S(1)} %get-tuple-element.50), channel_id=1, source_target_pairs={{0,30},{2,0},{4,2},{6,4},{8,6},{10,8},{12,10},{14,12},{16,14},{18,... | collective-permute-start | bytes 786440 | tf_op jit(solution)/shard_map/ppermute | solution.py:33

commit v3 on v2

--- a/solution.py
+++ b/solution.py
@@ -298,9 +298,10 @@
             dv_out[at, cols] = dv.astype(BF16)
     members = parts_ref.shape[0]
     width = parts_ref.shape[2]
-    sums = [parts_ref[i] for i in range(tp)]
-    for n in range(tp, members):
-        sums[n % tp] = sums[n % tp] + parts_ref[n]
+    each = members // tp
+    sums = [parts_ref[i * each] for i in range(tp)]
+    for n in range(1, each):
+        sums = [x + parts_ref[i * each + n] for i, x in enumerate(sums)]
     mine, total = sums[0], sums[0]
     for i in range(1, tp):
         mine = jnp.where(lax.axis_index("tp") == i, sums[i], mine)
@@ -352,7 +353,7 @@
         prev_v, p_prev, p_own, dp_own, do, qn, kn, pkn, qu, ku, pku, back_v, input_output_aliases={11: 1},
     )
     back = shifted(back, -1)
-    parts = lax.all_to_all(parts.reshape(members, 1, width), ("sp", "tp"), 0, 0)
+    parts = lax.all_to_all(parts.reshape(members, 1, width), ("tp", "sp"), 0, 0)
     d_queries, d_keys, d_values, d_table, d_gains = call(
         final_kernel, "final", (low, low, low, ((heads, ENTRIES), F32), ((2, HEAD_DIM), F32)),
         dq, dk_own, dv_own, back, qu, qr, ku, kr, g, parts,

time: 27.2 us -> 27.1 us (level)
  no operation moved by 1% of the time
where the time goes in v3:
time: 27.1 us; the launch traced here: 26.9 us
  blocking collectives  9.15 us (34%)
  waiting for transfers between devices  6.55 us (24%)
  starting transfers between devices  6.3 us (23%)
  Pallas kernels  4.23 us (16%)
  between operations  0.65 us (2%)
    all_to_all x1, blocking collectives, local(): parts = lax.all_to_all(parts.reshape(members, 1, width), ('tp', 'sp'), 0, 0)  9.15 us
    ppermute x3, waiting for transfers between devices, shifted(): lax.ppermute(block, 'sp', [(i, (i + distance) % size) for i in range(size)])  6.55 us
    ppermute x3, starting transfers between devices, shifted(): lax.ppermute(block, 'sp', [(i, (i + distance) % size) for i in range(size)])  6.3 us
    pallas_call x4, Pallas kernels, call(): pl.pallas_call(kernel, out_shape=tuple((place(*o) for o in outs)), **opti...  4.23 us
  transfers between devices with their start and end apart: 3, of which 2 were waited for; matrix products, arithmetic and copies ran while one was open for 0% of the time, Pallas kernels for 9%

profile of v3, /device:TPU:0, one launch (start us, length us, event | category | flops | bytes accessed | tf_op | source)
XLA Modules:
  0.0 26.9 jit_solution(17757301878801684997)
XLA Ops:
  0.6 3.0 %collective-permute-start.1 = (bf16[256,256]{1,0:T(8,128)(2,1)}, bf16[256,256]{1,0:T(8,128)(2,1)S(1)}, u32[]{:S(2)}, u32[]{:S(2)}) collective-permute-start(bf16[256,256]{1,0:T(8,128)(2,1)} %k_hbm.1), channel_id=1, source_target_pairs={{0,2},{2,4},{4,6},{6,8},{8,10},{10,12},{12,14},{14,16},{16,18},{18... | collective-permute-start | bytes 393224 | tf_op jit(solution)/shard_map/ppermute | solution.py:33
  3.7 1.5 %collective-permute-start = (bf16[256,256]{1,0:T(8,128)(2,1)}, bf16[256,256]{1,0:T(8,128)(2,1)S(1)}, u32[]{:S(2)}, u32[]{:S(2)}) collective-permute-start(bf16[256,256]{1,0:T(8,128)(2,1)} %v_hbm.1), channel_id=1, source_target_pairs={{0,2},{2,4},{4,6},{6,8},{8,10},{10,12},{12,14},{14,16},{16,18},{18... | collective-permute-start | bytes 393224 | tf_op jit(solution)/shard_map/ppermute | solution.py:33
  5.1 1.8 %shard_map.101 = (bf16[256,256]{1,0:T(8,128)(2,1)S(1)}, f32[2,128]{1,0:T(2,128)S(1)}, bf16[256,256]{1,0:T(8,128)(2,1)S(1)}, f32[256,256]{1,0:T(8,128)S(1)}, f32[...) custom-call(bf16[256,256]{1,0:T(8,128)(2,1)} %q_hbm.1, ...), custom_call_target="tpu_custom_call" | custom-call | tf_op jit(solution)/shard_map/pallas_call | solution.py:317
  7.0 5.2 %collective-permute-done.1.pk_ref = bf16[256,256]{1,0:T(8,128)(2,1)S(1)} collective-permute-done((bf16[256,256]{1,0:T(8,128)(2,1)}, bf16[256,256]{1,0:T(8,128)(2,1)S(1)}, u32[]{:S(2)}, u32[]{:S(2)}) %collective-permute-start.1) | collective-permute-done | bytes 131104 | tf_op jit(solution)/shard_map/ppermute | solution.py:33
  12.2 0.6 %shard_map.102 = (bf16[256,256]{1,0:T(8,128)(2,1)S(1)}, f32[256,256]{1,0:T(8,128)S(1)}, f32[2,3,128,128]{3,2,1,0:T(8,128)S(1)}, f32[2,3,128,128]{3,2,1,0:T(8,128...) custom-call(bf16[256,256]{1,0:T(8,128)(2,1)S(1)} %collective-permute-done.1.pk_ref, ...), custom_call_target="tpu_custom_call" | custom-call | tf_op jit(solution)/shard_map/pallas_call | solution.py:317
  12.8 1.3 %collective-permute-done.pv_ref = bf16[256,256]{1,0:T(8,128)(2,1)S(1)} collective-permute-done((bf16[256,256]{1,0:T(8,128)(2,1)}, bf16[256,256]{1,0:T(8,128)(2,1)S(1)}, u32[]{:S(2)}, u32[]{:S(2)}) %collective-permute-start) | collective-permute-done | bytes 131104 | tf_op jit(solution)/shard_map/ppermute | solution.py:33
  14.2 0.8 %shard_map.103 = (f32[256,256]{1,0:T(8,128)S(1)}, bf16[512,256]{1,0:T(8,128)(2,1)S(1)}, f32[256,256]{1,0:T(8,128)S(1)}, f32[160,128]{1,0:T(8,128)S(1)}) custom-call(bf16[256,256]{1,0:T(8,128)(2,1)S(1)} %collective-permute-done.pv_ref, f32[2,3,128,128]{3,2,1,0:T(8,128)S(1)} %get-tuple-element.38.pp_ref, ...), custom_call_target="tpu_custom_call", output_to_operand_aliasing={{1}: (11, {})} | custom-call | tf_op jit(solution)/shard_map/pallas_call | solution.py:317
  15.0 1.8 %collective-permute-start.2 = (bf16[512,256]{1,0:T(8,128)(2,1)S(1)}, bf16[512,256]{1,0:T(8,128)(2,1)S(1)}, u32[]{:S(2)}, u32[]{:S(2)}) collective-permute-start(bf16[512,256]{1,0:T(8,128)(2,1)S(1)} %get-tuple-element.50), channel_id=1, source_target_pairs={{0,30},{2,0},{4,2},{6,4},{8,6},{10,8},{12,10},{14,12},{16,14},{18,... | collective-permute-start | bytes 786440 | tf_op jit(solution)/shard_map/ppermute | solution.py:33
  16.7 9.1 %all_to_all.5.parts_ref = f32[32,1,640]{2,1,0:T(1,128)S(1)} all-to-all(f32[32,1,640]{2,1,0:T(1,128)S(1)} %bitcast.3), channel_id=1, replica_groups=mesh['sp'=16,'tp'=2] {'tp','sp'}, dimensions={0} | all-to-all | bytes 163840 | tf_op jit(solution)/shard_map/all_to_all | solution.py:356
  25.9 0.0 collective-permute-done.2.back_ref
  25.9 1.0 %shard_map.104 = (bf16[256,256]{1,0:T(8,128)(2,1)}, bf16[256,256]{1,0:T(8,128)(2,1)}, bf16[256,256]{1,0:T(8,128)(2,1)}, f32[2,192]{1,0:T(2,128)}, f32[2,128]{1,0:T(2,128)}) custom-call(f32[256,256]{1,0:T(8,128)S(1)} %get-tuple-element.47.dq_ref, f32[256,256]{1,0:T(8,128)S(1)} %get-tuple-element.48.dk_ref, f32[256,256]{1,0:T(8,128)S(1)} %get-tuple-element.49.dv_ref, ...), custom_call_target="tpu_custom_call" | custom-call | tf_op jit(solution)/shard_map/pallas_call | solution.py:317
Async XLA Ops:
  0.6 11.6 %collective-permute-start.1 = (bf16[256,256]{1,0:T(8,128)(2,1)}, bf16[256,256]{1,0:T(8,128)(2,1)S(1)}, u32[]{:S(2)}, u32[]{:S(2)}) collective-permute-start(bf16[256,256]{1,0:T(8,128)(2,1)} %k_hbm.1), channel_id=1, source_target_pairs={{0,2},{2,4},{4,6},{6,8},{8,10},{10,12},{12,14},{14,16},{16,18},{18... | collective-permute-start | bytes 393224 | tf_op jit(solution)/shard_map/ppermute | solution.py:33
  3.7 10.5 %collective-permute-start = (bf16[256,256]{1,0:T(8,128)(2,1)}, bf16[256,256]{1,0:T(8,128)(2,1)S(1)}, u32[]{:S(2)}, u32[]{:S(2)}) collective-permute-start(bf16[256,256]{1,0:T(8,128)(2,1)} %v_hbm.1), channel_id=1, source_target_pairs={{0,2},{2,4},{4,6},{6,8},{8,10},{10,12},{12,14},{14,16},{16,18},{18... | collective-permute-start | bytes 393224 | tf_op jit(solution)/shard_map/ppermute | solution.py:33
  15.0 10.9 %collective-permute-start.2 = (bf16[512,256]{1,0:T(8,128)(2,1)S(1)}, bf16[512,256]{1,0:T(8,128)(2,1)S(1)}, u32[]{:S(2)}, u32[]{:S(2)}) collective-permute-start(bf16[512,256]{1,0:T(8,128)(2,1)S(1)} %get-tuple-element.50), channel_id=1, source_target_pairs={{0,30},{2,0},{4,2},{6,4},{8,6},{10,8},{12,10},{14,12},{16,14},{18,... | collective-permute-start | bytes 786440 | tf_op jit(solution)/shard_map/ppermute | solution.py:33

commit v4 on v3

--- a/solution.py
+++ b/solution.py
@@ -296,12 +296,16 @@
                 dv = dv + back_ref[block_rows(PREV + from_end), cols].astype(F32)
             dk_out[at, cols] = rows_back(dk, ku_ref[at, cols], kr_ref[at, cols], gains_ref[1:2]).astype(BF16)
             dv_out[at, cols] = dv.astype(BF16)
-    members = parts_ref.shape[0]
-    width = parts_ref.shape[2]
-    each = members // tp
-    sums = [parts_ref[i * each] for i in range(tp)]
-    for n in range(1, each):
-        sums = [x + parts_ref[i * each + n] for i, x in enumerate(sums)]
+    lines = -(-heads * ENTRIES // HEAD_DIM) + 2
+    width = lines * HEAD_DIM
+    each, group = parts_ref.shape[0] // tp, 8 * lines
+    sums = []
+    for i in range(tp):
+        fold = parts_ref[i * each : i * each + group]
+        for r in range(group, each, group):
+            fold = fold + parts_ref[i * each + r : i * each + r + group]
+        rows_of = [sum(fold[n : n + 1] for n in range(c, group, lines)) for c in range(lines)]
+        sums.append(jnp.concatenate(rows_of, axis=1))
     mine, total = sums[0], sums[0]
     for i in range(1, tp):
         mine = jnp.where(lax.axis_index("tp") == i, sums[i], mine)
@@ -354,6 +358,7 @@
     )
     back = shifted(back, -1)
     parts = lax.all_to_all(parts.reshape(members, 1, width), ("tp", "sp"), 0, 0)
+    parts = parts.reshape(members * width // HEAD_DIM, HEAD_DIM)
     d_queries, d_keys, d_values, d_table, d_gains = call(
         final_kernel, "final", (low, low, low, ((heads, ENTRIES), F32), ((2, HEAD_DIM), F32)),
         dq, dk_own, dv_own, back, qu, qr, ku, kr, g, parts,

time: 27.1 us -> 27.1 us (level)
  no operation moved by 1% of the time
where the time goes in v4:
time: 27.1 us; the launch traced here: 26.9 us
  blocking collectives  9.15 us (34%)
  waiting for transfers between devices  6.55 us (24%)
  starting transfers between devices  6.3 us (23%)
  Pallas kernels  4.22 us (16%)
  between operations  0.65 us (2%)
    all_to_all x1, blocking collectives, local(): parts = lax.all_to_all(parts.reshape(members, 1, width), ('tp', 'sp'), 0, 0)  9.15 us
    ppermute x3, waiting for transfers between devices, shifted(): lax.ppermute(block, 'sp', [(i, (i + distance) % size) for i in range(size)])  6.55 us
    ppermute x3, starting transfers between devices, shifted(): lax.ppermute(block, 'sp', [(i, (i + distance) % size) for i in range(size)])  6.3 us
    pallas_call x4, Pallas kernels, call(): pl.pallas_call(kernel, out_shape=tuple((place(*o) for o in outs)), **opti...  4.22 us
  transfers between devices with their start and end apart: 3, of which 2 were waited for; matrix products, arithmetic and copies ran while one was open for 0% of the time, Pallas kernels for 9%

profile of v4, /device:TPU:0, one launch (start us, length us, event | category | flops | bytes accessed | tf_op | source)
XLA Modules:
  0.0 26.9 jit_solution(11553125669419998311)
XLA Ops:
  0.6 3.0 %collective-permute-start.1 = (bf16[256,256]{1,0:T(8,128)(2,1)}, bf16[256,256]{1,0:T(8,128)(2,1)S(1)}, u32[]{:S(2)}, u32[]{:S(2)}) collective-permute-start(bf16[256,256]{1,0:T(8,128)(2,1)} %k_hbm.1), channel_id=1, source_target_pairs={{0,2},{2,4},{4,6},{6,8},{8,10},{10,12},{12,14},{14,16},{16,18},{18... | collective-permute-start | bytes 393224 | tf_op jit(solution)/shard_map/ppermute | solution.py:33
  3.7 1.5 %collective-permute-start = (bf16[256,256]{1,0:T(8,128)(2,1)}, bf16[256,256]{1,0:T(8,128)(2,1)S(1)}, u32[]{:S(2)}, u32[]{:S(2)}) collective-permute-start(bf16[256,256]{1,0:T(8,128)(2,1)} %v_hbm.1), channel_id=1, source_target_pairs={{0,2},{2,4},{4,6},{6,8},{8,10},{10,12},{12,14},{14,16},{16,18},{18... | collective-permute-start | bytes 393224 | tf_op jit(solution)/shard_map/ppermute | solution.py:33
  5.1 1.8 %shard_map.101 = (bf16[256,256]{1,0:T(8,128)(2,1)S(1)}, f32[2,128]{1,0:T(2,128)S(1)}, bf16[256,256]{1,0:T(8,128)(2,1)S(1)}, f32[256,256]{1,0:T(8,128)S(1)}, f32[...) custom-call(bf16[256,256]{1,0:T(8,128)(2,1)} %q_hbm.1, ...), custom_call_target="tpu_custom_call" | custom-call | tf_op jit(solution)/shard_map/pallas_call | solution.py:321
  7.0 5.2 %collective-permute-done.1.pk_ref = bf16[256,256]{1,0:T(8,128)(2,1)S(1)} collective-permute-done((bf16[256,256]{1,0:T(8,128)(2,1)}, bf16[256,256]{1,0:T(8,128)(2,1)S(1)}, u32[]{:S(2)}, u32[]{:S(2)}) %collective-permute-start.1) | collective-permute-done | bytes 131104 | tf_op jit(solution)/shard_map/ppermute | solution.py:33
  12.2 0.6 %shard_map.102 = (bf16[256,256]{1,0:T(8,128)(2,1)S(1)}, f32[256,256]{1,0:T(8,128)S(1)}, f32[2,3,128,128]{3,2,1,0:T(8,128)S(1)}, f32[2,3,128,128]{3,2,1,0:T(8,128...) custom-call(bf16[256,256]{1,0:T(8,128)(2,1)S(1)} %collective-permute-done.1.pk_ref, ...), custom_call_target="tpu_custom_call" | custom-call | tf_op jit(solution)/shard_map/pallas_call | solution.py:321
  12.8 1.3 %collective-permute-done.pv_ref = bf16[256,256]{1,0:T(8,128)(2,1)S(1)} collective-permute-done((bf16[256,256]{1,0:T(8,128)(2,1)}, bf16[256,256]{1,0:T(8,128)(2,1)S(1)}, u32[]{:S(2)}, u32[]{:S(2)}) %collective-permute-start) | collective-permute-done | bytes 131104 | tf_op jit(solution)/shard_map/ppermute | solution.py:33
  14.2 0.8 %shard_map.103 = (f32[256,256]{1,0:T(8,128)S(1)}, bf16[512,256]{1,0:T(8,128)(2,1)S(1)}, f32[256,256]{1,0:T(8,128)S(1)}, f32[160,128]{1,0:T(8,128)S(1)}) custom-call(bf16[256,256]{1,0:T(8,128)(2,1)S(1)} %collective-permute-done.pv_ref, f32[2,3,128,128]{3,2,1,0:T(8,128)S(1)} %get-tuple-element.38.pp_ref, ...), custom_call_target="tpu_custom_call", output_to_operand_aliasing={{1}: (11, {})} | custom-call | tf_op jit(solution)/shard_map/pallas_call | solution.py:321
  15.0 1.8 %collective-permute-start.2 = (bf16[512,256]{1,0:T(8,128)(2,1)S(1)}, bf16[512,256]{1,0:T(8,128)(2,1)S(1)}, u32[]{:S(2)}, u32[]{:S(2)}) collective-permute-start(bf16[512,256]{1,0:T(8,128)(2,1)S(1)} %get-tuple-element.50), channel_id=1, source_target_pairs={{0,30},{2,0},{4,2},{6,4},{8,6},{10,8},{12,10},{14,12},{16,14},{18,... | collective-permute-start | bytes 786440 | tf_op jit(solution)/shard_map/ppermute | solution.py:33
  16.7 9.1 %all_to_all.5 = f32[32,1,640]{2,1,0:T(1,128)S(1)} all-to-all(f32[32,1,640]{2,1,0:T(1,128)S(1)} %bitcast.5), channel_id=1, replica_groups=mesh['sp'=16,'tp'=2] {'tp','sp'}, dimensions={0} | all-to-all | bytes 163840 | tf_op jit(solution)/shard_map/all_to_all | solution.py:360
  25.9 0.0 collective-permute-done.2.back_ref
  25.9 1.0 %shard_map.104 = (bf16[256,256]{1,0:T(8,128)(2,1)}, bf16[256,256]{1,0:T(8,128)(2,1)}, bf16[256,256]{1,0:T(8,128)(2,1)}, f32[2,192]{1,0:T(2,128)}, f32[2,128]{1,0:T(2,128)}) custom-call(f32[256,256]{1,0:T(8,128)S(1)} %get-tuple-element.47.dq_ref, f32[256,256]{1,0:T(8,128)S(1)} %get-tuple-element.48.dk_ref, f32[256,256]{1,0:T(8,128)S(1)} %get-tuple-element.49.dv_ref, ...), custom_call_target="tpu_custom_call" | custom-call | tf_op jit(solution)/shard_map/pallas_call | solution.py:321
Async XLA Ops:
  0.6 11.6 %collective-permute-start.1 = (bf16[256,256]{1,0:T(8,128)(2,1)}, bf16[256,256]{1,0:T(8,128)(2,1)S(1)}, u32[]{:S(2)}, u32[]{:S(2)}) collective-permute-start(bf16[256,256]{1,0:T(8,128)(2,1)} %k_hbm.1), channel_id=1, source_target_pairs={{0,2},{2,4},{4,6},{6,8},{8,10},{10,12},{12,14},{14,16},{16,18},{18... | collective-permute-start | bytes 393224 | tf_op jit(solution)/shard_map/ppermute | solution.py:33
  3.7 10.5 %collective-permute-start = (bf16[256,256]{1,0:T(8,128)(2,1)}, bf16[256,256]{1,0:T(8,128)(2,1)S(1)}, u32[]{:S(2)}, u32[]{:S(2)}) collective-permute-start(bf16[256,256]{1,0:T(8,128)(2,1)} %v_hbm.1), channel_id=1, source_target_pairs={{0,2},{2,4},{4,6},{6,8},{8,10},{10,12},{12,14},{14,16},{16,18},{18... | collective-permute-start | bytes 393224 | tf_op jit(solution)/shard_map/ppermute | solution.py:33
  15.0 10.9 %collective-permute-start.2 = (bf16[512,256]{1,0:T(8,128)(2,1)S(1)}, bf16[512,256]{1,0:T(8,128)(2,1)S(1)}, u32[]{:S(2)}, u32[]{:S(2)}) collective-permute-start(bf16[512,256]{1,0:T(8,128)(2,1)S(1)} %get-tuple-element.50), channel_id=1, source_target_pairs={{0,30},{2,0},{4,2},{6,4},{8,6},{10,8},{12,10},{14,12},{16,14},{18,... | collective-permute-start | bytes 786440 | tf_op jit(solution)/shard_map/ppermute | solution.py:33

commit v5 on v4

--- a/solution.py
+++ b/solution.py
@@ -156,8 +156,8 @@
 
 
 def keys_kernel(
-    pk_ref, qn_ref, do_ref, gains_ref, bias_ref, e_ref, stat_ref,
-    pkn_ref, pku_ref, pp_ref, po_ref, back_ref, dv_ref,
+    pk_ref, qn_ref, do_ref, gains_ref, bias_ref, e_ref, dp_ref, stat_ref,
+    pkn_ref, pku_ref, pp_ref, po_ref, both_ref, delta_ref, back_ref, dv_ref,
 ):
     rows, features = qn_ref.shape
     blocks = rows // BLOCK
@@ -187,6 +187,7 @@
         inverse = 1.0 / total
         scale = scale * inverse
         parts = []
+        delta = jnp.zeros((1, BLOCK), F32)
         for w in range(WINDOW):
             if p + w < PREV:
                 i = prev.index((p, w))
@@ -196,6 +197,10 @@
                 i = own.index((p, w))
                 parts.append(e_ref[h, i] * scale)
                 po_ref[h, i] = parts[w]
+                both = parts[w] * dp_ref[h, i]
+                both_ref[h, i] = both
+                delta = delta + jnp.sum(both, axis=0, keepdims=True)
+        delta_ref[h, p : p + 1] = delta
         prob[h, p] = jnp.concatenate([x.astype(BF16) for x in parts], axis=0)
     dv = [[None] * (blocks + PREV) for _ in range(heads)]
     for h, p in cells:
@@ -210,7 +215,7 @@
 
 
 def values_kernel(
-    pv_ref, pp_ref, po_ref, dpo_ref, do_ref, qn_ref, kn_ref, pkn_ref, qu_ref, ku_ref, pku_ref, _,
+    pv_ref, pp_ref, po_ref, both_ref, delta_ref, do_ref, qn_ref, kn_ref, pkn_ref, qu_ref, ku_ref, pku_ref, _,
     dq_ref, back_ref, dk_ref, parts_ref,
 ):
     rows, features = qn_ref.shape
@@ -224,19 +229,18 @@
         if any(pp == p for pp, _ in prev):
             new[h, p] = dot(pv_ref[p * BLOCK :, columns(h)], do_ref[block_rows(p), columns(h)], (1, 1))
     for h, p in cells:
-        probs, d_probs, n = [], [], 0
+        delta = delta_ref[h, p : p + 1]
+        d_score[h, p] = [None] * WINDOW
         for w in range(WINDOW):
             if p + w < PREV:
-                i = prev.index((p, w))
-                probs.append(pp_ref[h, i])
-                d_probs.append(new[h, p][block_rows(n)])
-                n += 1
+                d_prob = new[h, p][block_rows(w)]
+                delta = delta + jnp.sum(pp_ref[h, prev.index((p, w))] * d_prob, axis=0, keepdims=True)
+        for w in range(WINDOW):
+            if p + w < PREV:
+                d_score[h, p][w] = pp_ref[h, prev.index((p, w))] * (new[h, p][block_rows(w)] - delta)
             else:
                 i = own.index((p, w))
-                probs.append(po_ref[h, i])
-                d_probs.append(dpo_ref[h, i])
-        delta = sum(jnp.sum(a * b, axis=0, keepdims=True) for a, b in zip(probs, d_probs))
-        d_score[h, p] = [a * (b - delta) for a, b in zip(probs, d_probs)]
+                d_score[h, p][w] = both_ref[h, i] - po_ref[h, i] * delta
         d_low[h, p] = jnp.concatenate([d.astype(BF16) for d in d_score[h, p]], axis=0)
     dk = [[None] * (blocks + PREV) for _ in range(heads)]
     for h, p in cells:
@@ -348,13 +352,13 @@
         scratch_shapes=[pltpu.VMEM(*low)] * 3
         + [pltpu.VMEM((heads, ENTRIES), F32), pltpu.SemaphoreType.DMA((6,))],
     )
-    pkn, pku, p_prev, p_own, back_v, dv_own = call(
-        keys_kernel, "keys", (tail_low, tail, tiles(prev), tiles(own), ((2 * TAIL, features), BF16), wide),
-        prev_k, qn, do, g, bias, e_own, stats,
+    pkn, pku, p_prev, p_own, both, delta_own, back_v, dv_own = call(
+        keys_kernel, "keys", (tail_low, tail, tiles(prev), tiles(own), tiles(own), ((heads, blocks, BLOCK), F32), ((2 * TAIL, features), BF16), wide),
+        prev_k, qn, do, g, bias, e_own, dp_own, stats,
     )
     dq, back, dk_own, parts = call(
         values_kernel, "values", (wide, ((2 * TAIL, features), BF16), wide, ((members * width // HEAD_DIM, HEAD_DIM), F32)),
-        prev_v, p_prev, p_own, dp_own, do, qn, kn, pkn, qu, ku, pku, back_v, input_output_aliases={11: 1},
+        prev_v, p_prev, p_own, both, delta_own, do, qn, kn, pkn, qu, ku, pku, back_v, input_output_aliases={12: 1},
     )
     back = shifted(back, -1)
     parts = lax.all_to_all(parts.reshape(members, 1, width), ("tp", "sp"), 0, 0)

time: 27.1 us -> 27.1 us (level)
  no operation moved by 1% of the time
where the time goes in v5:
time: 27.1 us; the launch traced here: 26.9 us
  blocking collectives  9.15 us (34%)
  waiting for transfers between devices  6.52 us (24%)
  starting transfers between devices  6.31 us (23%)
  Pallas kernels  4.31 us (16%)
  between operations  0.65 us (2%)
    all_to_all x1, blocking collectives, local(): parts = lax.all_to_all(parts.reshape(members, 1, width), ('tp', 'sp'), 0, 0)  9.15 us
    ppermute x3, waiting for transfers between devices, shifted(): lax.ppermute(block, 'sp', [(i, (i + distance) % size) for i in range(size)])  6.52 us
    ppermute x3, starting transfers between devices, shifted(): lax.ppermute(block, 'sp', [(i, (i + distance) % size) for i in range(size)])  6.31 us
    pallas_call x4, Pallas kernels, call(): pl.pallas_call(kernel, out_shape=tuple((place(*o) for o in outs)), **opti...  4.31 us
  transfers between devices with their start and end apart: 3, of which 2 were waited for; matrix products, arithmetic and copies ran while one was open for 0% of the time, Pallas kernels for 9%

profile of v5, /device:TPU:0, one launch (start us, length us, event | category | flops | bytes accessed | tf_op | source)
XLA Modules:
  0.0 26.9 jit_solution(8598882896006972861)
XLA Ops:
  0.6 3.0 %collective-permute-start.1 = (bf16[256,256]{1,0:T(8,128)(2,1)}, bf16[256,256]{1,0:T(8,128)(2,1)S(1)}, u32[]{:S(2)}, u32[]{:S(2)}) collective-permute-start(bf16[256,256]{1,0:T(8,128)(2,1)} %k_hbm.1), channel_id=1, source_target_pairs={{0,2},{2,4},{4,6},{6,8},{8,10},{10,12},{12,14},{14,16},{16,18},{18... | collective-permute-start | bytes 393224 | tf_op jit(solution)/shard_map/ppermute | solution.py:33
  3.7 1.5 %collective-permute-start = (bf16[256,256]{1,0:T(8,128)(2,1)}, bf16[256,256]{1,0:T(8,128)(2,1)S(1)}, u32[]{:S(2)}, u32[]{:S(2)}) collective-permute-start(bf16[256,256]{1,0:T(8,128)(2,1)} %v_hbm.1), channel_id=1, source_target_pairs={{0,2},{2,4},{4,6},{6,8},{8,10},{10,12},{12,14},{14,16},{16,18},{18... | collective-permute-start | bytes 393224 | tf_op jit(solution)/shard_map/ppermute | solution.py:33
  5.1 1.8 %shard_map.101 = (bf16[256,256]{1,0:T(8,128)(2,1)S(1)}, f32[2,128]{1,0:T(2,128)S(1)}, bf16[256,256]{1,0:T(8,128)(2,1)S(1)}, f32[256,256]{1,0:T(8,128)S(1)}, f32[...) custom-call(bf16[256,256]{1,0:T(8,128)(2,1)} %q_hbm.1, ...), custom_call_target="tpu_custom_call" | custom-call | tf_op jit(solution)/shard_map/pallas_call | solution.py:325
  7.0 5.2 %collective-permute-done.1.pk_ref = bf16[256,256]{1,0:T(8,128)(2,1)S(1)} collective-permute-done((bf16[256,256]{1,0:T(8,128)(2,1)}, bf16[256,256]{1,0:T(8,128)(2,1)S(1)}, u32[]{:S(2)}, u32[]{:S(2)}) %collective-permute-start.1) | collective-permute-done | bytes 131104 | tf_op jit(solution)/shard_map/ppermute | solution.py:33
  12.2 0.6 %shard_map.102 = (bf16[256,256]{1,0:T(8,128)(2,1)S(1)}, f32[256,256]{1,0:T(8,128)S(1)}, f32[2,3,128,128]{3,2,1,0:T(8,128)S(1)}, f32[2,3,128,128]{3,2,1,0:T(8,128...) custom-call(bf16[256,256]{1,0:T(8,128)(2,1)S(1)} %collective-permute, ...), custom_call_target="tpu_custom_call" | custom-call | tf_op jit(solution)/shard_map/pallas_call | solution.py:325
  12.9 1.3 %collective-permute-done.pv_ref = bf16[256,256]{1,0:T(8,128)(2,1)S(1)} collective-permute-done((bf16[256,256]{1,0:T(8,128)(2,1)}, bf16[256,256]{1,0:T(8,128)(2,1)S(1)}, u32[]{:S(2)}, u32[]{:S(2)}) %collective-permute-start) | collective-permute-done | bytes 131104 | tf_op jit(solution)/shard_map/ppermute | solution.py:33
  14.2 0.8 %shard_map.103 = (f32[256,256]{1,0:T(8,128)S(1)}, bf16[512,256]{1,0:T(8,128)(2,1)S(1)}, f32[256,256]{1,0:T(8,128)S(1)}, f32[160,128]{1,0:T(8,128)S(1)}) custom-call(bf16[256,256]{1,0:T(8,128)(2,1)S(1)} %collective-permute-done.pv_ref, f32[2,3,128,128]{3,2,1,0:T(8,128)S(1)} %get-tuple-element.41.pp_ref, ...), custom_call_target="tpu_custom_call", output_to_operand_aliasing={{1}: (12, {})} | custom-call | tf_op jit(solution)/shard_map/pallas_call | solution.py:325
  15.0 1.8 %collective-permute-start.2 = (bf16[512,256]{1,0:T(8,128)(2,1)S(1)}, bf16[512,256]{1,0:T(8,128)(2,1)S(1)}, u32[]{:S(2)}, u32[]{:S(2)}) collective-permute-start(bf16[512,256]{1,0:T(8,128)(2,1)S(1)} %get-tuple-element.54), channel_id=1, source_target_pairs={{0,30},{2,0},{4,2},{6,4},{8,6},{10,8},{12,10},{14,12},{16,14},{18,... | collective-permute-start | bytes 786440 | tf_op jit(solution)/shard_map/ppermute | solution.py:33
  16.8 9.1 %all_to_all.5 = f32[32,1,640]{2,1,0:T(1,128)S(1)} all-to-all(f32[32,1,640]{2,1,0:T(1,128)S(1)} %bitcast.5), channel_id=1, replica_groups=mesh['sp'=16,'tp'=2] {'tp','sp'}, dimensions={0} | all-to-all | bytes 163840 | tf_op jit(solution)/shard_map/all_to_all | solution.py:364
  25.9 0.0 collective-permute-done.2.back_ref
  25.9 1.0 %shard_map.104 = (bf16[256,256]{1,0:T(8,128)(2,1)}, bf16[256,256]{1,0:T(8,128)(2,1)}, bf16[256,256]{1,0:T(8,128)(2,1)}, f32[2,192]{1,0:T(2,128)}, f32[2,128]{1,0:T(2,128)}) custom-call(f32[256,256]{1,0:T(8,128)S(1)} %get-tuple-element.51.dq_ref, f32[256,256]{1,0:T(8,128)S(1)} %get-tuple-element.52.dk_ref, f32[256,256]{1,0:T(8,128)S(1)} %get-tuple-element.53.dv_ref, ...), custom_call_target="tpu_custom_call" | custom-call | tf_op jit(solution)/shard_map/pallas_call | solution.py:325
Async XLA Ops:
  0.6 11.6 %collective-permute-start.1 = (bf16[256,256]{1,0:T(8,128)(2,1)}, bf16[256,256]{1,0:T(8,128)(2,1)S(1)}, u32[]{:S(2)}, u32[]{:S(2)}) collective-permute-start(bf16[256,256]{1,0:T(8,128)(2,1)} %k_hbm.1), channel_id=1, source_target_pairs={{0,2},{2,4},{4,6},{6,8},{8,10},{10,12},{12,14},{14,16},{16,18},{18... | collective-permute-start | bytes 393224 | tf_op jit(solution)/shard_map/ppermute | solution.py:33
  3.7 10.5 %collective-permute-start = (bf16[256,256]{1,0:T(8,128)(2,1)}, bf16[256,256]{1,0:T(8,128)(2,1)S(1)}, u32[]{:S(2)}, u32[]{:S(2)}) collective-permute-start(bf16[256,256]{1,0:T(8,128)(2,1)} %v_hbm.1), channel_id=1, source_target_pairs={{0,2},{2,4},{4,6},{6,8},{8,10},{10,12},{12,14},{14,16},{16,18},{18... | collective-permute-start | bytes 393224 | tf_op jit(solution)/shard_map/ppermute | solution.py:33
  15.0 10.9 %collective-permute-start.2 = (bf16[512,256]{1,0:T(8,128)(2,1)S(1)}, bf16[512,256]{1,0:T(8,128)(2,1)S(1)}, u32[]{:S(2)}, u32[]{:S(2)}) collective-permute-start(bf16[512,256]{1,0:T(8,128)(2,1)S(1)} %get-tuple-element.54), channel_id=1, source_target_pairs={{0,30},{2,0},{4,2},{6,4},{8,6},{10,8},{12,10},{14,12},{16,14},{18,... | collective-permute-start | bytes 786440 | tf_op jit(solution)/shard_map/ppermute | solution.py:33
